TPU v7x, 32 devices: a whole 2x2x4 slice. The times are simulated.
32 devices in a mesh: sp: 2 (over x), dp: 16 (over z, y, core).
Axes of the slice: x: 2, y: 2, z: 4, core: 2. Of those that a mesh axis runs over, the one named last changes fastest.
Arguments:
- hidden_in: bfloat16 [1024, 2048], P('sp'), may hold values from -6 to 6
- content_weight: bfloat16 [2048, 2048], P('sp', 'dp'), may hold values from -0.125 to 0.125
- gating_weight: bfloat16 [2048, 2048], P('sp', 'dp'), may hold values from -2 to 2
- norm_gain: float32 [2048], P('dp'), may hold values from 0.1 to 1.9
- mixing_weight: bfloat16 [16, 128, 128], P('dp'), may hold values from -0.5 to 0.5
- mixing_bias: float32 [16, 128], P('dp'), may hold values from 0.1 to 1.9
- out_grad: bfloat16 [1024, 2048], P('sp', 'dp'), may hold values from -13 to 13
Outputs:
- input_grad: bfloat16 [1024, 2048], P('sp', 'dp')
- content_grad: float32 [2048, 2048], P('sp', 'dp')
- gating_grad: float32 [2048, 2048], P('sp', 'dp')
- mixing_grad: float32 [16, 128, 128], P('dp')
All inputs are finite; a program needn't handle non-finite values.
Results may differ from a plain program's by a relative error of at most 0.019.
Values may be sent and summed in bfloat16 or wider, within the bound.
A program may use at most 64 MiB of HBM per device.

v0:
```python
import functools
import math

import jax
import jax.numpy as jnp
from jax import lax
from jax.experimental import pallas as pl
from jax.experimental.pallas import tpu as pltpu
from jax.sharding import PartitionSpec as P

GROUP_DIM = 128
BLOCK = 128


norm_eps = 1e-05


def gelu_slope(values):
    cumulative = 0.5 * (1.0 + lax.erf(values * (1.0 / math.sqrt(2.0))))
    density = jnp.exp(-0.5 * values * values) * (1.0 / math.sqrt(2.0 * math.pi))
    return cumulative + values * density


def causal_table(weights):
    row_ids = lax.broadcasted_iota(jnp.int32, (BLOCK, BLOCK), 0)
    col_ids = lax.broadcasted_iota(jnp.int32, (BLOCK, BLOCK), 1)
    keeper = (col_ids <= row_ids)[None]
    return (jnp.where(keeper, weights, jnp.zeros_like(weights)), keeper)


def hidden_term(hidden_in, grads):
    return lax.dot_general(
        hidden_in, grads, (((0,), (0,)), ((), ())), preferred_element_type=jnp.float32
    )


def local(
    hidden_in, content_weight, gating_weight, norm_gain, mixing_weight, mixing_bias, out_grad
):
    tok_rows = hidden_in.shape[0]
    local_width = content_weight.shape[1]
    groups_here = local_width // GROUP_DIM
    blocks = tok_rows // BLOCK
    full_width = local_width * lax.axis_size("dp")
    grad_scale = 1.0 / math.sqrt(tok_rows * lax.axis_size("sp"))
    whole_content, whole_gating = (
        lax.all_gather(content_weight, "sp", axis=0, tiled=True),
        lax.all_gather(gating_weight, "sp", axis=0, tiled=True),
    )
    joined_weight = jnp.concatenate([whole_content, whole_gating], axis=1)
    pre_both = jnp.dot(hidden_in, joined_weight, preferred_element_type=jnp.float32).astype(
        jnp.bfloat16
    )
    pre_content = pre_both[:, :local_width].astype(jnp.float32)
    pre_gating = pre_both[:, local_width:].astype(jnp.float32)
    content = jax.nn.gelu(pre_content, approximate=False)
    gating = jax.nn.gelu(pre_gating, approximate=False)
    spatial, keeper = causal_table(mixing_weight)
    grad_wide = out_grad.astype(jnp.float32)
    mixed_grad = (grad_wide * content).astype(jnp.bfloat16)
    mixed_blocks = mixed_grad.reshape(blocks, BLOCK, groups_here, GROUP_DIM)
    normed_grad = jnp.einsum(
        "gts,btgc->bsgc", spatial, mixed_blocks, preferred_element_type=jnp.float32
    )
    centred_grad = normed_grad.reshape(tok_rows, local_width) * norm_gain[None, :]
    row_sum, row_square, grad_sum, grad_raw = lax.psum(
        (
            jnp.sum(gating, axis=1),
            jnp.sum(gating * gating, axis=1),
            jnp.sum(centred_grad, axis=1),
            jnp.sum(centred_grad * gating, axis=1),
        ),
        "dp",
    )
    row_mean = (row_sum / full_width)[:, None]
    row_var = (row_square / full_width)[:, None] - row_mean * row_mean
    inv_std = lax.rsqrt(row_var + norm_eps)
    centred = (gating - row_mean) * inv_std
    first_moment = (grad_sum / full_width)[:, None]
    second_moment = inv_std * ((grad_raw / full_width)[:, None] - row_mean * first_moment)
    normed = (centred * norm_gain[None, :]).astype(jnp.bfloat16)
    normed_blocks = normed.reshape(blocks, BLOCK, groups_here, GROUP_DIM)
    mixed = jnp.einsum("gts,bsgc->btgc", spatial, normed_blocks, preferred_element_type=jnp.float32)
    mixed = (mixed + jnp.transpose(mixing_bias)[None, :, :, None]).reshape(tok_rows, local_width)
    content_pre_grad = (grad_wide * mixed * gelu_slope(pre_content)).astype(jnp.bfloat16)
    local_mixing = jnp.einsum(
        "btgc,bsgc->gts", mixed_blocks, normed_blocks, preferred_element_type=jnp.float32
    )
    local_mixing = jnp.where(keeper, local_mixing, 0.0)
    mixing_grad = lax.psum(local_mixing.astype(jnp.bfloat16), "sp").astype(jnp.float32) * grad_scale
    gating_back = inv_std * (centred_grad - first_moment - centred * second_moment)
    gating_pre_grad = (gating_back * gelu_slope(pre_gating)).astype(jnp.bfloat16)
    joined_grad = jnp.concatenate([content_pre_grad, gating_pre_grad], axis=1)
    partial_input = lax.dot_general(
        joined_grad, joined_weight, (((1,), (1,)), ((), ())), preferred_element_type=jnp.float32
    )
    input_grad = lax.psum_scatter(
        partial_input.astype(jnp.bfloat16), "dp", scatter_dimension=1, tiled=True
    )
    both_grads = (
        lax.psum_scatter(
            hidden_term(hidden_in, joined_grad).astype(jnp.bfloat16),
            "sp",
            scatter_dimension=0,
            tiled=True,
        ).astype(jnp.float32)
        * grad_scale
    )
    content_grad = both_grads[:, :local_width]
    gating_grad = both_grads[:, local_width:]
    return (input_grad, content_grad, gating_grad, mixing_grad)


def phi_and_slope(values):
    cumulative = 0.5 * (1.0 + lax.erf(values * (1.0 / math.sqrt(2.0))))
    density = jnp.exp(-0.5 * values * values) * (1.0 / math.sqrt(2.0 * math.pi))
    return cumulative, cumulative + values * density


def dot(a, b, ca, cb):
    return lax.dot_general(
        a, b, (((ca,), (cb,)), ((), ())), preferred_element_type=jnp.float32
    )


def fused_kernel(
    n_dp, full_width, grad_scale,
    h_in, wc_in, wg_in, gain_in, mix_in, bias_in, og_in,
    x_out, c_out, g_out, m_out,
    gain_ref, mix_ref, bias_ref, hid, hid_t, wts, og, cg, cg_t, cs, gat, slope_g, mg, joined,
    stat_a, stat_quad, stat_b, stat_z,
    part, r_core, q_send, r_y, z_send, r_z, acc,
    gs, gr, go, ms, mr,
    load_sem, w_send, w_recv, sq_send, sq_recv, sz_send, sz_recv,
    core_send, core_recv, y_send, y_recv, zz_send, zz_recv,
    gx_send, gx_recv, mx_send, mx_recv, out_sem, x_buf, m_buf,
):
    toks = hid.shape[0]
    chunks = toks // BLOCK
    shard = wc_in.shape[0]
    nz = n_dp // 4
    half = toks // 2
    tiles = gs.shape[0]
    tile = gs.shape[1]
    bf16 = jnp.bfloat16
    f32 = jnp.float32

    i = lax.axis_index("sp")
    j = lax.axis_index("dp")
    x_peer = 1 - i
    c = lax.rem(j, 2)
    y = lax.rem(j // 2, 2)
    z = j // 4
    j_core = j + 1 - 2 * c
    j_y = j + 2 - 4 * y
    j_diag = j_core + 2 - 4 * y

    mid = lax.rem((z + 1) // 2, 2)
    z_xor = (z, z + 1 - 2 * lax.rem(z, 2), z + 2 - 4 * (z // 2), 3 - z)

    def z_dev(q):
        return z_xor[q] * 4 + y * 2 + c

    def dev(a, b):
        return {"sp": a, "dp": b}

    def remote(src, dst, ssem, rsem, target):
        return pltpu.make_async_remote_copy(
            src_ref=src, dst_ref=dst, send_sem=ssem, recv_sem=rsem,
            device_id=target, device_id_type=pl.DeviceIdType.MESH,
        )

    mine = pl.multiple_of(i * shard, shard)
    theirs = pl.multiple_of(x_peer * shard, shard)
    loads = [
        pltpu.make_async_copy(wc_in, wts.at[pl.ds(mine, shard), pl.ds(0, BLOCK)], load_sem.at[0]),
        pltpu.make_async_copy(h_in, hid, load_sem.at[1]),
        pltpu.make_async_copy(wg_in, wts.at[pl.ds(mine, shard), pl.ds(BLOCK, BLOCK)], load_sem.at[2]),
        pltpu.make_async_copy(og_in, og, load_sem.at[3]),
        pltpu.make_async_copy(gain_in, gain_ref, load_sem.at[4]),
        pltpu.make_async_copy(mix_in, mix_ref, load_sem.at[5]),
        pltpu.make_async_copy(bias_in, bias_ref, load_sem.at[6]),
    ]
    for load in loads:
        load.start()

    barrier = pltpu.get_barrier_semaphore()
    peers = [dev(x_peer, j), dev(i, j_core), dev(i, j_y), dev(i, j_diag)]
    peers += [dev(i, z_dev(q)) for q in range(1, nz)]
    for peer in peers:
        pl.semaphore_signal(barrier, inc=1, device_id=peer, device_id_type=pl.DeviceIdType.MESH)
    pl.semaphore_wait(barrier, len(peers))

    pieces = w_send.shape[0] // 2
    piece = shard // pieces
    w_copies = []
    for which, src in ((0, wc_in), (1, wg_in)):
        for p in range(pieces):
            copy = remote(
                src.at[pl.ds(p * piece, piece), :],
                wts.at[pl.ds(pl.multiple_of(mine + p * piece, piece), piece), pl.ds(which * BLOCK, BLOCK)],
                w_send.at[which * pieces + p], w_recv.at[which * pieces + p],
                dev(x_peer, j),
            )
            copy.start()
            w_copies.append(copy)

    keep = lax.broadcasted_iota(jnp.int32, (BLOCK, BLOCK), 1) <= lax.broadcasted_iota(
        jnp.int32, (BLOCK, BLOCK), 0
    )
    for load in loads:
        load.wait()
    spatial = jnp.where(keep, mix_ref[0].astype(f32), 0.0).astype(bf16)
    gain = gain_ref[...]
    bias = jnp.broadcast_to(bias_ref[...], (BLOCK, BLOCK)).T
    own = dot(hid[:, pl.ds(mine, shard)], wts[pl.ds(mine, shard), :], 1, 0)
    joined_pre = own
    acc_c = go.at[pl.ds(0, toks), pl.ds(0, BLOCK)]
    acc_g = go.at[pl.ds(0, toks), pl.ds(BLOCK, BLOCK)]
    go[pl.ds(0, toks), :] = joined_pre
    for b in range(hid.shape[1] // BLOCK):
        hid_t[pl.ds(b * BLOCK, BLOCK), :] = hid[:, pl.ds(b * BLOCK, BLOCK)].T

    def finish(which, target):
        for p in range(pieces):
            w_copies[which * pieces + p].wait_recv()
            at = pl.multiple_of(theirs + p * piece, piece)
            target[...] += dot(
                hid[:, pl.ds(at, piece)], wts[pl.ds(at, piece), pl.ds(which * BLOCK, BLOCK)], 1, 0
            )

    finish(0, acc_c)
    for k in range(chunks):
        rows = pl.ds(k * BLOCK, BLOCK)
        pre = go[rows, 0:BLOCK].astype(bf16).astype(f32)
        wide = og[rows, :].astype(f32)
        cumulative, slope = phi_and_slope(pre)
        cs[rows, :] = wide * slope
        mixed_grad = (wide * (pre * cumulative)).astype(bf16)
        mg[rows, :] = mixed_grad
        centred_grad = dot(spatial, mixed_grad, 0, 0) * gain
        cg[rows, :] = centred_grad
        cg_t[rows, :] = centred_grad.T

    finish(1, acc_g)
    for k in range(chunks):
        rows = pl.ds(k * BLOCK, BLOCK)
        pre = go[rows, BLOCK:2 * BLOCK].astype(bf16).astype(f32)
        cumulative, slope = phi_and_slope(pre)
        gating = pre * cumulative
        gat[rows, :] = gating
        slope_g[rows, :] = slope
        turned = gating.T
        grad_turned = cg_t[rows, :]
        base = 4 * (k * BLOCK // half)
        cols = pl.ds(k * BLOCK % half, BLOCK)
        for row, table in enumerate((turned, turned * turned, grad_turned, grad_turned * turned)):
            stat_a[base + row:base + row + 1, cols] = jnp.sum(table, axis=0, keepdims=True)

    stat_copies = []
    for s, target in enumerate((j_core, j_y, j_diag)):
        copy = remote(stat_a, stat_quad.at[s], sq_send.at[s], sq_recv.at[s], dev(i, target))
        copy.start()
        stat_copies.append(copy)
    for copy in stat_copies:
        copy.wait()
    stat_b[...] = (stat_a[...] + stat_quad[0]) + (stat_quad[1] + stat_quad[2])
    stat_copies = []
    for q in range(1, nz):
        copy = remote(
            stat_b, stat_z.at[q - 1], sz_send.at[q - 1], sz_recv.at[q - 1], dev(i, z_dev(q))
        )
        copy.start()
        stat_copies.append(copy)
    for copy in stat_copies:
        copy.wait()
    total = stat_b[...]
    for q in range(1, nz):
        total = total + stat_z[q - 1]
    total = total * (1.0 / full_width)

    mixing = jnp.zeros((BLOCK, BLOCK), f32)
    for k in range(chunks):
        rows = pl.ds(k * BLOCK, BLOCK)
        base = 4 * (k * BLOCK // half)
        col = k * BLOCK % half
        part_of = total[base:base + 4, col:col + BLOCK]
        mean = part_of[0:1]
        inv = lax.rsqrt(part_of[1:2] - mean * mean + norm_eps)
        first = part_of[2:3]
        second = inv * (part_of[3:4] - mean * first)

        def spread(row):
            return jnp.broadcast_to(row, (BLOCK, BLOCK)).T

        inv_w = spread(inv)
        centred = (gat[rows, :] - spread(mean)) * inv_w
        normed = (centred * gain).astype(bf16)
        mixed = dot(spatial, normed, 1, 0) + bias
        joined[rows, 0:BLOCK] = (cs[rows, :] * mixed).astype(bf16)
        back = inv_w * (cg[rows, :] - spread(first) - centred * spread(second))
        joined[rows, BLOCK:2 * BLOCK] = (back * slope_g[rows, :]).astype(bf16)
        mixing = mixing + dot(mg[rows, :], normed, 1, 1)
    mixing = jnp.where(keep, mixing, 0.0)

    waits = []
    stores = []

    def store(src, dst):
        copy = pltpu.make_async_copy(src, dst, out_sem.at[len(stores)])
        copy.start()
        stores.append(copy)

    order = [(slot, h) for slot in range(nz) for h in range(2)]
    pieces_in = len(order)

    def input_part(n):
        slot, h = order[n]
        grads = joined[pl.ds(h * half, half), :]
        at = pl.multiple_of(z_xor[3 - slot] * (4 * BLOCK), 4 * BLOCK)
        res = dot(grads, wts[pl.ds(at, 4 * BLOCK), :], 1, 1).astype(bf16)
        for yy in range(2):
            for cc in range(2):
                at = (yy * 2 + cc) * BLOCK
                part[n, cc, yy] = res[:, at:at + BLOCK]
        copy = remote(part.at[n, 1 - c], r_core.at[n], core_send.at[n], core_recv.at[n], dev(i, j_core))
        copy.start()
        waits.append(copy)
        core_copies[n] = copy

    def weight_part(t):
        at = pl.multiple_of(theirs + t * tile, tile)
        gs[t] = dot(hid_t[pl.ds(at, tile), :], joined[...], 1, 0).astype(bf16)
        copy = remote(gs.at[t], gr.at[t], gx_send.at[t], gx_recv.at[t], dev(x_peer, j))
        copy.start()
        waits.append(copy)
        return copy

    core_copies, y_copies, z_copies, g_copies = {}, {}, {}, {}

    def second_stage(n):
        core_copies[n].wait_recv()
        q_send[n] = (part[n, c, 1 - y].astype(f32) + r_core[n, 1 - y].astype(f32)).astype(bf16)
        copy = remote(q_send.at[n], r_y.at[n], y_send.at[n], y_recv.at[n], dev(i, j_y))
        copy.start()
        waits.append(copy)
        y_copies[n] = copy

    def direct(h):
        return remote(z_send.at[0, h], r_z.at[0, h], zz_send.at[0, h], zz_recv.at[0, h], dev(i, z_dev(3)))

    def relay(h):
        return remote(z_send.at[0, h], r_z.at[3, h], zz_send.at[0, h], zz_recv.at[3, h], dev(i, z_dev(1)))

    def third_stage(n):
        slot, h = order[n]
        y_copies[n].wait_recv()
        res = (part[n, c, y].astype(f32) + r_core[n, y].astype(f32)) + r_y[n].astype(f32)
        if slot == nz - 1:
            acc[h] = res
            return
        if slot == 0:
            z_send[0, h] = res.astype(bf16)

            @pl.when(mid == 1)
            def _():
                direct(h).start()

            @pl.when(mid == 0)
            def _():
                relay(h).start()

            waits.append(direct(h))
            return
        if slot == 1:

            @pl.when(mid == 1)
            def _():
                relay(h).wait_recv()
                z_send[1, h] = (res + r_z[3, h].astype(f32)).astype(bf16)

            @pl.when(mid == 0)
            def _():
                z_send[1, h] = res.astype(bf16)
        else:
            z_send[slot, h] = res.astype(bf16)
        copy = remote(
            z_send.at[slot, h], r_z.at[slot, h], zz_send.at[slot, h], zz_recv.at[slot, h], dev(i, z_dev(3 - slot))
        )
        copy.start()
        waits.append(copy)
        z_copies[slot, h] = copy

    def last_stage(h):
        @pl.when(mid == 1)
        def _():
            direct(h).wait_recv()
            acc[h] = acc[h] + r_z[0, h].astype(f32)

        res = acc[h]
        for slot in range(1, nz - 1):
            z_copies[slot, h].wait_recv()
            res = res + r_z[slot, h].astype(f32)
        x_buf[pl.ds(h * half, half), :] = res.astype(bf16)
        store(x_buf.at[pl.ds(h * half, half), :], x_out.at[pl.ds(h * half, half), :])

    for step in range(pieces_in + 2):
        if step < pieces_in:
            input_part(step)
        if step < tiles:
            g_copies[step] = weight_part(step)
        if step >= 2:
            second_stage(step - 2)
    ms[...] = mixing.astype(bf16)
    m_copy = remote(ms, mr, mx_send, mx_recv, dev(x_peer, j))
    m_copy.start()
    waits.append(m_copy)
    for t in range(tiles):
        at = pl.multiple_of(mine + t * tile, tile)
        go[pl.ds(t * tile, tile), :] = dot(hid_t[pl.ds(at, tile), :], joined[...], 1, 0)
    for n in range(pieces_in):
        third_stage(n)
    for t in range(tiles):
        g_copies[t].wait_recv()
        rows = pl.ds(t * tile, tile)
        go[rows, :] = (go[rows, :] + gr[t].astype(f32)) * grad_scale
        store(go.at[rows, pl.ds(0, BLOCK)], c_out.at[rows, :])
        store(go.at[rows, pl.ds(BLOCK, BLOCK)], g_out.at[rows, :])
    m_copy.wait_recv()
    m_buf[0] = (mixing + mr[...].astype(f32)) * grad_scale
    store(m_buf, m_out)
    for h in range(2):
        last_stage(h)
    for copy in stores:
        copy.wait()
    for copy in w_copies + waits:
        copy.wait_send()


def store_kernel(*refs):
    count = len(refs) // 3
    src, dst, held = refs[:count], refs[count:2 * count], refs[2 * count:3 * count]
    sem = refs[-1]
    loads = [pltpu.make_async_copy(src[k], held[k], sem.at[0, k]) for k in range(count)]
    stores = [pltpu.make_async_copy(held[k], dst[k], sem.at[1, k]) for k in range(count)]
    for load in loads:
        load.start()
    for load, store in zip(loads, stores):
        load.wait()
        store.start()
    for store in stores:
        store.wait()


def fused(n_dp, hidden_in, content_weight, gating_weight, norm_gain, mixing_weight, mixing_bias, out_grad):
    toks, depth = hidden_in.shape
    shard, width = content_weight.shape
    half = toks // 2
    nz = n_dp // 4
    tile = 256
    tiles = shard // tile
    pieces = 2
    grad_scale = 1.0 / math.sqrt(2 * toks)
    bf16, f32 = jnp.bfloat16, jnp.float32
    in_hbm = pl.BlockSpec(memory_space=pltpu.HBM)
    dma = pltpu.SemaphoreType.DMA
    V = pltpu.VMEM
    scratch = [
        V((1, width), f32), V((1, BLOCK, BLOCK), bf16), V((1, BLOCK), f32),
        V((toks, depth), bf16), V((depth, toks), bf16), V((depth, 2 * width), bf16), V((toks, width), bf16),
        V((toks, width), f32), V((toks, width), f32), V((toks, width), f32), V((toks, width), f32),
        V((toks, width), f32), V((toks, width), bf16), V((toks, 2 * width), bf16),
        V((8, toks // 2), f32), V((3, 8, toks // 2), f32), V((8, toks // 2), f32), V((nz - 1, 8, toks // 2), f32),
        V((2 * nz, 2, 2, half, width), bf16), V((2 * nz, 2, half, width), bf16),
        V((2 * nz, half, width), bf16), V((2 * nz, half, width), bf16),
        V((nz - 1, 2, half, width), bf16), V((nz, 2, half, width), bf16), V((2, half, width), f32),
        V((tiles, tile, 2 * width), bf16), V((tiles, tile, 2 * width), bf16), V((shard, 2 * width), f32),
        V((BLOCK, BLOCK), bf16), V((BLOCK, BLOCK), bf16),
        dma((7,)), dma((2 * pieces,)), dma((2 * pieces,)), dma((3,)), dma((3,)), dma((nz - 1,)), dma((nz - 1,)),
        dma((2 * nz,)), dma((2 * nz,)), dma((2 * nz,)), dma((2 * nz,)), dma((nz - 1, 2)), dma((nz, 2)),
        dma((tiles,)), dma((tiles,)), dma, dma, dma((2 * tiles + 3,)),
        V((toks, width), bf16), V((1, BLOCK, BLOCK), f32),
    ]
    results = pl.pallas_call(
        functools.partial(fused_kernel, n_dp, width * n_dp, grad_scale),
        out_shape=(
            jax.ShapeDtypeStruct((toks, width), bf16),
            jax.ShapeDtypeStruct((shard, width), f32),
            jax.ShapeDtypeStruct((shard, width), f32),
            jax.ShapeDtypeStruct(mixing_weight.shape, f32),
        ),
        in_specs=[in_hbm] * 7,
        out_specs=(in_hbm,) * 4,
        scratch_shapes=scratch,
        compiler_params=pltpu.CompilerParams(
            collective_id=0, has_side_effects=True, vmem_limit_bytes=67043328
        ),
    )(hidden_in, content_weight, gating_weight, norm_gain[None, :], mixing_weight, mixing_bias, out_grad)
    return pl.pallas_call(
        store_kernel,
        out_shape=tuple(jax.ShapeDtypeStruct(r.shape, r.dtype) for r in results),
        in_specs=[in_hbm] * 4,
        out_specs=(in_hbm,) * 4,
        scratch_shapes=[V(r.shape, r.dtype) for r in results] + [dma((2, 4))],
        compiler_params=pltpu.CompilerParams(vmem_limit_bytes=67043328),
    )(*results)


def fits(n_sp, n_dp, toks, shard, width):
    paired = n_sp == 2 and n_dp == 16
    return paired and width == GROUP_DIM and shard % 512 == 0 and toks % (2 * BLOCK) == 0 and toks <= shard


def solve(*args):
    n_sp, n_dp = lax.axis_size("sp"), lax.axis_size("dp")
    shard, width = args[1].shape
    if fits(n_sp, n_dp, args[0].shape[0], shard, width) and args[0].shape[1] == n_dp * width:
        return fused(n_dp, *args)
    return local(*args)


def solution(mesh):
    in_specs = (
        P("sp", None),
        P("sp", "dp"),
        P("sp", "dp"),
        P("dp"),
        P("dp", None, None),
        P("dp", None),
        P("sp", "dp"),
    )
    out_specs = (P("sp", "dp"), P("sp", "dp"), P("sp", "dp"), P("dp", None, None))
    return jax.shard_map(solve, mesh=mesh, in_specs=in_specs, out_specs=out_specs, check_vma=False)
```

profile of v0, /device:TPU:0, one launch (start us, length us, event | category | flops | bytes accessed | tf_op | source)
XLA Modules:
  0.0 47.1 jit_solution(3372002332692115637)
XLA Ops:
  0.6 44.3 %shard_map.102 = (bf16[512,128]{1,0:T(8,128)(2,1)}, f32[1024,128]{1,0:T(8,128)}, f32[1024,128]{1,0:T(8,128)}, f32[1,128,128]{2,1,0:T(8,128)}) custom-call(bf16[512,2048]{1,0:T(8,128)(2,1)} %h_in.1, bf16[1024,128]{1,0:T(8,128)(2,1)} %wc_in.1, bf16[1024,128]{1,0:T(8,128)(2,1)} %wg_in.1, f32[1,128]{1,0:T(1,128)} %bitcast.1, bf16[1,128,128]{2,1,0:T(8,128)(2,1)} %mix_in.1, ...), custom_call_target="tpu_custom_call" | custom-call | tf_op jit(solution)/shard_map/pallas_call | solution.py:484
  45.0 2.2 %shard_map.103 = (bf16[512,128]{1,0:T(8,128)(2,1)}, f32[1024,128]{1,0:T(8,128)}, f32[1024,128]{1,0:T(8,128)}, f32[1,128,128]{2,1,0:T(8,128)}) custom-call(bf16[512,128]{1,0:T(8,128)(2,1)} %get-tuple-element.8.refs_0_, f32[1024,128]{1,0:T(8,128)} %get-tuple-element.9.refs_1_, f32[1024,128]{1,0:T(8,128)} %get-tuple-element.10.refs_2_, ...), custom_call_target="tpu_custom_call" | custom-call | tf_op jit(solution)/shard_map/pallas_call | solution.py:499
where the time goes:
time: 47.3 us; the launch traced here: 47.1 us
  Pallas kernels  46.5 us (98%)
  between operations  0.64 us (1%)
    pallas_call x1, Pallas kernels, fused(): pl.pallas_call(functools.partial(fused_kernel, n_dp, width * n_dp, grad_s...  44.3 us
    pallas_call x1, Pallas kernels, fused(): pl.pallas_call(store_kernel, out_shape=tuple((jax.ShapeDtypeStruct(r.shap...  2.16 us

commit v1 on v0

--- a/solution.py
+++ b/solution.py
@@ -133,7 +133,7 @@
     gs, gr, go, ms, mr,
     load_sem, w_send, w_recv, sq_send, sq_recv, sz_send, sz_recv,
     core_send, core_recv, y_send, y_recv, zz_send, zz_recv,
-    gx_send, gx_recv, mx_send, mx_recv, out_sem, x_buf, m_buf,
+    gx_send, gx_recv, mx_send, mx_recv,
 ):
     toks = hid.shape[0]
     chunks = toks // BLOCK
@@ -304,12 +304,6 @@
     mixing = jnp.where(keep, mixing, 0.0)
 
     waits = []
-    stores = []
-
-    def store(src, dst):
-        copy = pltpu.make_async_copy(src, dst, out_sem.at[len(stores)])
-        copy.start()
-        stores.append(copy)
 
     order = [(slot, h) for slot in range(nz) for h in range(2)]
     pieces_in = len(order)
@@ -401,8 +395,7 @@
         for slot in range(1, nz - 1):
             z_copies[slot, h].wait_recv()
             res = res + r_z[slot, h].astype(f32)
-        x_buf[pl.ds(h * half, half), :] = res.astype(bf16)
-        store(x_buf.at[pl.ds(h * half, half), :], x_out.at[pl.ds(h * half, half), :])
+        x_out[pl.ds(h * half, half), :] = res.astype(bf16)
 
     for step in range(pieces_in + 2):
         if step < pieces_in:
@@ -423,30 +416,22 @@
     for t in range(tiles):
         g_copies[t].wait_recv()
         rows = pl.ds(t * tile, tile)
-        go[rows, :] = (go[rows, :] + gr[t].astype(f32)) * grad_scale
-        store(go.at[rows, pl.ds(0, BLOCK)], c_out.at[rows, :])
-        store(go.at[rows, pl.ds(BLOCK, BLOCK)], g_out.at[rows, :])
+        done = (go[rows, :] + gr[t].astype(f32)) * grad_scale
+        c_out[rows, :] = done[:, 0:BLOCK]
+        g_out[rows, :] = done[:, BLOCK:2 * BLOCK]
     m_copy.wait_recv()
-    m_buf[0] = (mixing + mr[...].astype(f32)) * grad_scale
-    store(m_buf, m_out)
+    m_out[0] = (mixing + mr[...].astype(f32)) * grad_scale
     for h in range(2):
         last_stage(h)
-    for copy in stores:
-        copy.wait()
     for copy in w_copies + waits:
         copy.wait_send()
 
 
 def store_kernel(*refs):
-    count = len(refs) // 3
-    src, dst, held = refs[:count], refs[count:2 * count], refs[2 * count:3 * count]
-    sem = refs[-1]
-    loads = [pltpu.make_async_copy(src[k], held[k], sem.at[0, k]) for k in range(count)]
-    stores = [pltpu.make_async_copy(held[k], dst[k], sem.at[1, k]) for k in range(count)]
-    for load in loads:
-        load.start()
-    for load, store in zip(loads, stores):
-        load.wait()
+    count = len(refs) // 2
+    src, dst, sem = refs[:count], refs[count:2 * count], refs[-1]
+    stores = [pltpu.make_async_copy(src[k], dst[k], sem.at[k]) for k in range(count)]
+    for store in stores:
         store.start()
     for store in stores:
         store.wait()
@@ -478,32 +463,30 @@
         V((BLOCK, BLOCK), bf16), V((BLOCK, BLOCK), bf16),
         dma((7,)), dma((2 * pieces,)), dma((2 * pieces,)), dma((3,)), dma((3,)), dma((nz - 1,)), dma((nz - 1,)),
         dma((2 * nz,)), dma((2 * nz,)), dma((2 * nz,)), dma((2 * nz,)), dma((nz - 1, 2)), dma((nz, 2)),
-        dma((tiles,)), dma((tiles,)), dma, dma, dma((2 * tiles + 3,)),
-        V((toks, width), bf16), V((1, BLOCK, BLOCK), f32),
+        dma((tiles,)), dma((tiles,)), dma, dma,
     ]
     results = pl.pallas_call(
         functools.partial(fused_kernel, n_dp, width * n_dp, grad_scale),
         out_shape=(
-            jax.ShapeDtypeStruct((toks, width), bf16),
-            jax.ShapeDtypeStruct((shard, width), f32),
-            jax.ShapeDtypeStruct((shard, width), f32),
-            jax.ShapeDtypeStruct(mixing_weight.shape, f32),
+            V((toks, width), bf16),
+            V((shard, width), f32),
+            V((shard, width), f32),
+            V(mixing_weight.shape, f32),
         ),
         in_specs=[in_hbm] * 7,
-        out_specs=(in_hbm,) * 4,
+        out_specs=(pl.BlockSpec(memory_space=pltpu.VMEM),) * 4,
         scratch_shapes=scratch,
         compiler_params=pltpu.CompilerParams(
-            collective_id=0, has_side_effects=True, vmem_limit_bytes=67043328
+            collective_id=0, has_side_effects=True, vmem_limit_bytes=60*1024*1024
         ),
     )(hidden_in, content_weight, gating_weight, norm_gain[None, :], mixing_weight, mixing_bias, out_grad)
     return pl.pallas_call(
         store_kernel,
         out_shape=tuple(jax.ShapeDtypeStruct(r.shape, r.dtype) for r in results),
-        in_specs=[in_hbm] * 4,
+        in_specs=[pl.BlockSpec(memory_space=pltpu.VMEM)] * 4,
         out_specs=(in_hbm,) * 4,
-        scratch_shapes=[V(r.shape, r.dtype) for r in results] + [dma((2, 4))],
-        compiler_params=pltpu.CompilerParams(vmem_limit_bytes=67043328),
-    )(*results)
+        scratch_shapes=[dma((4,))],
+    )(*[pltpu.with_memory_space_constraint(r, pltpu.VMEM) for r in results])
 
 
 def fits(n_sp, n_dp, toks, shard, width):

time: 47.3 us -> 45.5 us (0.962)
  Pallas kernels: 46.5 us -> 44.7 us
    pallas_call x1, Pallas kernels: 2.16 us -> 1.06 us  [fused(): pl.pallas_call(store_kernel, out_shape=tuple((jax.ShapeDtypeStruct(r.shap...]
    pallas_call x1, Pallas kernels: 44.3 us -> 43.6 us  [fused(): pl.pallas_call(functools.partial(fused_kernel, n_dp, width * n_dp, grad_s...]
where the time goes in v1:
time: 45.5 us; the launch traced here: 45.3 us
  Pallas kernels  44.7 us (98%)
  between operations  0.64 us (1%)
    pallas_call x1, Pallas kernels, fused(): pl.pallas_call(functools.partial(fused_kernel, n_dp, width * n_dp, grad_s...  43.6 us
    pallas_call x1, Pallas kernels, fused(): pl.pallas_call(store_kernel, out_shape=tuple((jax.ShapeDtypeStruct(r.shap...  1.06 us

profile of v1, /device:TPU:0, one launch (start us, length us, event | category | flops | bytes accessed | tf_op | source)
XLA Modules:
  0.0 45.3 jit_solution(18015531934692063211)
XLA Ops:
  0.6 43.6 %shard_map.102 = (bf16[512,128]{1,0:T(8,128)(2,1)S(1)}, f32[1024,128]{1,0:T(8,128)S(1)}, f32[1024,128]{1,0:T(8,128)S(1)}, f32[1,128,128]{2,1,0:T(8,128)S(1)}) custom-call(bf16[512,2048]{1,0:T(8,128)(2,1)} %h_in.1, bf16[1024,128]{1,0:T(8,128)(2,1)} %wc_in.1, bf16[1024,128]{1,0:T(8,128)(2,1)} %wg_in.1, f32[1,128]{1,0:T(1,128)} %bitcast.1, ...), custom_call_target="tpu_custom_call" | custom-call | tf_op jit(solution)/shard_map/pallas_call | solution.py:468
  44.3 1.1 %shard_map.103 = (bf16[512,128]{1,0:T(8,128)(2,1)}, f32[1024,128]{1,0:T(8,128)}, f32[1024,128]{1,0:T(8,128)}, f32[1,128,128]{2,1,0:T(8,128)}) custom-call(bf16[512,128]{1,0:T(8,128)(2,1)S(1)} %get-tuple-element.8.refs_0_, f32[1024,128]{1,0:T(8,128)S(1)} %get-tuple-element.9.refs_1_, f32[1024,128]{1,0:T(8,128)S(1)} %get-tuple-element.10.refs_2_, ...), custom_call_target="tpu_custom_call" | custom-call | tf_op jit(solution)/shard_map/pallas_call | solution.py:483

commit v2 on v1

--- a/solution.py
+++ b/solution.py
@@ -128,10 +128,10 @@
     h_in, wc_in, wg_in, gain_in, mix_in, bias_in, og_in,
     x_out, c_out, g_out, m_out,
     gain_ref, mix_ref, bias_ref, hid, hid_t, wts, og, cg, cg_t, cs, gat, slope_g, mg, joined,
-    stat_a, stat_quad, stat_b, stat_z,
+    stat_a, stat_r,
     part, r_core, q_send, r_y, z_send, r_z, acc,
     gs, gr, go, ms, mr,
-    load_sem, w_send, w_recv, sq_send, sq_recv, sz_send, sz_recv,
+    load_sem, w_send, w_recv, st_send, st_recv, hello,
     core_send, core_recv, y_send, y_recv, zz_send, zz_recv,
     gx_send, gx_recv, mx_send, mx_recv,
 ):
@@ -184,12 +184,23 @@
     for load in loads:
         load.start()
 
+    def tell(sem, target):
+        pl.semaphore_signal(sem, inc=1, device_id=target, device_id_type=pl.DeviceIdType.MESH)
+
     barrier = pltpu.get_barrier_semaphore()
-    peers = [dev(x_peer, j), dev(i, j_core), dev(i, j_y), dev(i, j_diag)]
-    peers += [dev(i, z_dev(q)) for q in range(1, nz)]
-    for peer in peers:
-        pl.semaphore_signal(barrier, inc=1, device_id=peer, device_id_type=pl.DeviceIdType.MESH)
-    pl.semaphore_wait(barrier, len(peers))
+
+    @pl.when(i == 0)
+    def _():
+        tell(barrier, dev(x_peer, j))
+
+    @pl.when(i == 1)
+    def _():
+        pl.semaphore_wait(barrier, 1)
+        tell(hello, dev(x_peer, j))
+
+    @pl.when(i == 0)
+    def _():
+        pl.semaphore_wait(hello, 1)
 
     pieces = w_send.shape[0] // 2
     piece = shard // pieces
@@ -204,6 +215,19 @@
             )
             copy.start()
             w_copies.append(copy)
+
+    others = [dev(i, lax.rem(j + k, n_dp)) for k in range(1, n_dp)]
+
+    @pl.when(i == 0)
+    def _():
+        for target in others:
+            tell(barrier, target)
+        pl.semaphore_wait(barrier, len(others))
+        tell(hello, dev(x_peer, j))
+
+    @pl.when(i == 1)
+    def _():
+        pl.semaphore_wait(hello, 1)
 
     keep = lax.broadcasted_iota(jnp.int32, (BLOCK, BLOCK), 1) <= lax.broadcasted_iota(
         jnp.int32, (BLOCK, BLOCK), 0
@@ -258,25 +282,14 @@
             stat_a[base + row:base + row + 1, cols] = jnp.sum(table, axis=0, keepdims=True)
 
     stat_copies = []
-    for s, target in enumerate((j_core, j_y, j_diag)):
-        copy = remote(stat_a, stat_quad.at[s], sq_send.at[s], sq_recv.at[s], dev(i, target))
+    for k, target in enumerate(others):
+        copy = remote(stat_a, stat_r.at[k], st_send.at[k], st_recv.at[k], target)
         copy.start()
         stat_copies.append(copy)
-    for copy in stat_copies:
-        copy.wait()
-    stat_b[...] = (stat_a[...] + stat_quad[0]) + (stat_quad[1] + stat_quad[2])
-    stat_copies = []
-    for q in range(1, nz):
-        copy = remote(
-            stat_b, stat_z.at[q - 1], sz_send.at[q - 1], sz_recv.at[q - 1], dev(i, z_dev(q))
-        )
-        copy.start()
-        stat_copies.append(copy)
-    for copy in stat_copies:
-        copy.wait()
-    total = stat_b[...]
-    for q in range(1, nz):
-        total = total + stat_z[q - 1]
+    total = stat_a[...]
+    for k, copy in enumerate(stat_copies):
+        copy.wait_recv()
+        total = total + stat_r[k]
     total = total * (1.0 / full_width)
 
     mixing = jnp.zeros((BLOCK, BLOCK), f32)
@@ -303,7 +316,7 @@
         mixing = mixing + dot(mg[rows, :], normed, 1, 1)
     mixing = jnp.where(keep, mixing, 0.0)
 
-    waits = []
+    waits = stat_copies
 
     order = [(slot, h) for slot in range(nz) for h in range(2)]
     pieces_in = len(order)
@@ -455,13 +468,13 @@
         V((toks, depth), bf16), V((depth, toks), bf16), V((depth, 2 * width), bf16), V((toks, width), bf16),
         V((toks, width), f32), V((toks, width), f32), V((toks, width), f32), V((toks, width), f32),
         V((toks, width), f32), V((toks, width), bf16), V((toks, 2 * width), bf16),
-        V((8, toks // 2), f32), V((3, 8, toks // 2), f32), V((8, toks // 2), f32), V((nz - 1, 8, toks // 2), f32),
+        V((8, toks // 2), f32), V((n_dp - 1, 8, toks // 2), f32),
         V((2 * nz, 2, 2, half, width), bf16), V((2 * nz, 2, half, width), bf16),
         V((2 * nz, half, width), bf16), V((2 * nz, half, width), bf16),
         V((nz - 1, 2, half, width), bf16), V((nz, 2, half, width), bf16), V((2, half, width), f32),
         V((tiles, tile, 2 * width), bf16), V((tiles, tile, 2 * width), bf16), V((shard, 2 * width), f32),
         V((BLOCK, BLOCK), bf16), V((BLOCK, BLOCK), bf16),
-        dma((7,)), dma((2 * pieces,)), dma((2 * pieces,)), dma((3,)), dma((3,)), dma((nz - 1,)), dma((nz - 1,)),
+        dma((7,)), dma((2 * pieces,)), dma((2 * pieces,)), dma((n_dp - 1,)), dma((n_dp - 1,)), pltpu.SemaphoreType.REGULAR,
         dma((2 * nz,)), dma((2 * nz,)), dma((2 * nz,)), dma((2 * nz,)), dma((nz - 1, 2)), dma((nz, 2)),
         dma((tiles,)), dma((tiles,)), dma, dma,
     ]

time: 45.5 us -> 43.1 us (0.947)
  Pallas kernels: 44.7 us -> 42.3 us
    pallas_call x1, Pallas kernels: 43.6 us -> 41.2 us  [fused(): pl.pallas_call(functools.partial(fused_kernel, n_dp, width * n_dp, grad_s...]
where the time goes in v2:
time: 43.1 us; the launch traced here: 42.9 us
  Pallas kernels  42.3 us (98%)
  between operations  0.64 us (1%)
    pallas_call x1, Pallas kernels, fused(): pl.pallas_call(functools.partial(fused_kernel, n_dp, width * n_dp, grad_s...  41.2 us
    pallas_call x1, Pallas kernels, fused(): pl.pallas_call(store_kernel, out_shape=tuple((jax.ShapeDtypeStruct(r.shap...  1.06 us

profile of v2, /device:TPU:0, one launch (start us, length us, event | category | flops | bytes accessed | tf_op | source)
XLA Modules:
  0.0 42.9 jit_solution(9619129104965869294)
XLA Ops:
  0.6 41.2 %shard_map.102 = (bf16[512,128]{1,0:T(8,128)(2,1)S(1)}, f32[1024,128]{1,0:T(8,128)S(1)}, f32[1024,128]{1,0:T(8,128)S(1)}, f32[1,128,128]{2,1,0:T(8,128)S(1)}) custom-call(bf16[512,2048]{1,0:T(8,128)(2,1)} %h_in.1, bf16[1024,128]{1,0:T(8,128)(2,1)} %wc_in.1, bf16[1024,128]{1,0:T(8,128)(2,1)} %wg_in.1, f32[1,128]{1,0:T(1,128)} %bitcast.1, ...), custom_call_target="tpu_custom_call" | custom-call | tf_op jit(solution)/shard_map/pallas_call | solution.py:481
  41.9 1.1 %shard_map.103 = (bf16[512,128]{1,0:T(8,128)(2,1)}, f32[1024,128]{1,0:T(8,128)}, f32[1024,128]{1,0:T(8,128)}, f32[1,128,128]{2,1,0:T(8,128)}) custom-call(bf16[512,128]{1,0:T(8,128)(2,1)S(1)} %get-tuple-element.8.refs_0_, f32[1024,128]{1,0:T(8,128)S(1)} %get-tuple-element.9.refs_1_, f32[1024,128]{1,0:T(8,128)S(1)} %get-tuple-element.10.refs_2_, ...), custom_call_target="tpu_custom_call" | custom-call | tf_op jit(solution)/shard_map/pallas_call | solution.py:496

commit v3 on v2

v3 whole, which is shorter than its diff:
```python
import functools
import math

import jax
import jax.numpy as jnp
from jax import lax
from jax.experimental import pallas as pl
from jax.experimental.pallas import tpu as pltpu
from jax.sharding import PartitionSpec as P

GROUP_DIM = 128
BLOCK = 128


norm_eps = 1e-05


def gelu_slope(values):
    cumulative = 0.5 * (1.0 + lax.erf(values * (1.0 / math.sqrt(2.0))))
    density = jnp.exp(-0.5 * values * values) * (1.0 / math.sqrt(2.0 * math.pi))
    return cumulative + values * density


def causal_table(weights):
    row_ids = lax.broadcasted_iota(jnp.int32, (BLOCK, BLOCK), 0)
    col_ids = lax.broadcasted_iota(jnp.int32, (BLOCK, BLOCK), 1)
    keeper = (col_ids <= row_ids)[None]
    return (jnp.where(keeper, weights, jnp.zeros_like(weights)), keeper)


def hidden_term(hidden_in, grads):
    return lax.dot_general(
        hidden_in, grads, (((0,), (0,)), ((), ())), preferred_element_type=jnp.float32
    )


def local(
    hidden_in, content_weight, gating_weight, norm_gain, mixing_weight, mixing_bias, out_grad
):
    tok_rows = hidden_in.shape[0]
    local_width = content_weight.shape[1]
    groups_here = local_width // GROUP_DIM
    blocks = tok_rows // BLOCK
    full_width = local_width * lax.axis_size("dp")
    grad_scale = 1.0 / math.sqrt(tok_rows * lax.axis_size("sp"))
    whole_content, whole_gating = (
        lax.all_gather(content_weight, "sp", axis=0, tiled=True),
        lax.all_gather(gating_weight, "sp", axis=0, tiled=True),
    )
    joined_weight = jnp.concatenate([whole_content, whole_gating], axis=1)
    pre_both = jnp.dot(hidden_in, joined_weight, preferred_element_type=jnp.float32).astype(
        jnp.bfloat16
    )
    pre_content = pre_both[:, :local_width].astype(jnp.float32)
    pre_gating = pre_both[:, local_width:].astype(jnp.float32)
    content = jax.nn.gelu(pre_content, approximate=False)
    gating = jax.nn.gelu(pre_gating, approximate=False)
    spatial, keeper = causal_table(mixing_weight)
    grad_wide = out_grad.astype(jnp.float32)
    mixed_grad = (grad_wide * content).astype(jnp.bfloat16)
    mixed_blocks = mixed_grad.reshape(blocks, BLOCK, groups_here, GROUP_DIM)
    normed_grad = jnp.einsum(
        "gts,btgc->bsgc", spatial, mixed_blocks, preferred_element_type=jnp.float32
    )
    centred_grad = normed_grad.reshape(tok_rows, local_width) * norm_gain[None, :]
    row_sum, row_square, grad_sum, grad_raw = lax.psum(
        (
            jnp.sum(gating, axis=1),
            jnp.sum(gating * gating, axis=1),
            jnp.sum(centred_grad, axis=1),
            jnp.sum(centred_grad * gating, axis=1),
        ),
        "dp",
    )
    row_mean = (row_sum / full_width)[:, None]
    row_var = (row_square / full_width)[:, None] - row_mean * row_mean
    inv_std = lax.rsqrt(row_var + norm_eps)
    centred = (gating - row_mean) * inv_std
    first_moment = (grad_sum / full_width)[:, None]
    second_moment = inv_std * ((grad_raw / full_width)[:, None] - row_mean * first_moment)
    normed = (centred * norm_gain[None, :]).astype(jnp.bfloat16)
    normed_blocks = normed.reshape(blocks, BLOCK, groups_here, GROUP_DIM)
    mixed = jnp.einsum("gts,bsgc->btgc", spatial, normed_blocks, preferred_element_type=jnp.float32)
    mixed = (mixed + jnp.transpose(mixing_bias)[None, :, :, None]).reshape(tok_rows, local_width)
    content_pre_grad = (grad_wide * mixed * gelu_slope(pre_content)).astype(jnp.bfloat16)
    local_mixing = jnp.einsum(
        "btgc,bsgc->gts", mixed_blocks, normed_blocks, preferred_element_type=jnp.float32
    )
    local_mixing = jnp.where(keeper, local_mixing, 0.0)
    mixing_grad = lax.psum(local_mixing.astype(jnp.bfloat16), "sp").astype(jnp.float32) * grad_scale
    gating_back = inv_std * (centred_grad - first_moment - centred * second_moment)
    gating_pre_grad = (gating_back * gelu_slope(pre_gating)).astype(jnp.bfloat16)
    joined_grad = jnp.concatenate([content_pre_grad, gating_pre_grad], axis=1)
    partial_input = lax.dot_general(
        joined_grad, joined_weight, (((1,), (1,)), ((), ())), preferred_element_type=jnp.float32
    )
    input_grad = lax.psum_scatter(
        partial_input.astype(jnp.bfloat16), "dp", scatter_dimension=1, tiled=True
    )
    both_grads = (
        lax.psum_scatter(
            hidden_term(hidden_in, joined_grad).astype(jnp.bfloat16),
            "sp",
            scatter_dimension=0,
            tiled=True,
        ).astype(jnp.float32)
        * grad_scale
    )
    content_grad = both_grads[:, :local_width]
    gating_grad = both_grads[:, local_width:]
    return (input_grad, content_grad, gating_grad, mixing_grad)


def phi_and_slope(values):
    cumulative = 0.5 * (1.0 + lax.erf(values * (1.0 / math.sqrt(2.0))))
    density = jnp.exp(-0.5 * values * values) * (1.0 / math.sqrt(2.0 * math.pi))
    return cumulative, cumulative + values * density


def dot(a, b, ca, cb):
    return lax.dot_general(
        a, b, (((ca,), (cb,)), ((), ())), preferred_element_type=jnp.float32
    )


def fused_kernel(
    n_dp, full_width, grad_scale,
    h_in, wc_in, wg_in, gain_in, mix_in, bias_in, og_in,
    x_out, c_out, g_out, m_out,
    gain_ref, mix_ref, bias_ref, hid, hid_t, wts, wq, og, pre_acc,
    cs, gat, gat_t, slope_g, mg, cg, centred_ref, eq, part,
    s1, r1, s2, r2, z_send, r_z, gs, gr,
    load_sem, hello, quad_ok, all_ok, w_send, w_recv, q_send, q_recv, a_send, a_recv,
    e_send, c_recv, yg_recv, sg_recv, gx_send, gx_recv, zz_send, zz_recv, relay_recv,
):
    toks = hid.shape[0]
    chunks = toks // BLOCK
    nz = n_dp // 4
    zs = nz // 2
    shard = zs * 4 * BLOCK
    tile = shard // chunks
    bf16 = jnp.bfloat16
    f32 = jnp.float32

    i = lax.axis_index("sp")
    j = lax.axis_index("dp")
    x_peer = 1 - i
    c = lax.rem(j, 2)
    y = lax.rem(j // 2, 2)
    z = j // 4
    me = y * 2 + c
    y_mate = (1 - y) * 2 + c
    mates = (y * 2 + 1 - c, y_mate, (1 - y) * 2 + 1 - c)

    mid = lax.rem((z + 1) // 2, 2)
    z_xor = (z, z + 1 - 2 * lax.rem(z, 2), z + 2 - 4 * (z // 2), 3 - z)

    def dev(a, b):
        return {"sp": a, "dp": b}

    def mate_dev(rel):
        return dev(i, z * 4 + mates[rel])

    def z_dev(q):
        return dev(i, z_xor[q] * 4 + me)

    def remote(src, dst, ssem, rsem, target):
        return pltpu.make_async_remote_copy(
            src_ref=src, dst_ref=dst, send_sem=ssem, recv_sem=rsem,
            device_id=target, device_id_type=pl.DeviceIdType.MESH,
        )

    def send(*args):
        remote(*args).start()

    def await_bytes(ref, sem):
        pltpu.make_async_copy(ref, ref, sem).wait()

    def tell(sem, target):
        pl.semaphore_signal(sem, inc=1, device_id=target, device_id_type=pl.DeviceIdType.MESH)

    x_dev = dev(x_peer, j)
    my_z = pl.ds(zs * i, zs)
    their_z = pl.ds(zs * x_peer, zs)
    mine = pl.multiple_of(i * shard, shard)
    theirs = pl.multiple_of(x_peer * shard, shard)
    loads = [
        pltpu.make_async_copy(wg_in, wts.at[1, my_z], load_sem.at[0]),
        pltpu.make_async_copy(wc_in, wts.at[0, my_z], load_sem.at[1]),
        pltpu.make_async_copy(h_in, hid, load_sem.at[2]),
        pltpu.make_async_copy(og_in, og, load_sem.at[3]),
        pltpu.make_async_copy(gain_in, gain_ref, load_sem.at[4]),
        pltpu.make_async_copy(mix_in, mix_ref, load_sem.at[5]),
        pltpu.make_async_copy(bias_in, bias_ref, load_sem.at[6]),
    ]
    for load in loads:
        load.start()

    barrier = pltpu.get_barrier_semaphore()
    lead = i == 0
    follow = i == 1
    herald = jnp.logical_and(lead, me == 1)
    plain = jnp.logical_and(lead, me != 1)

    @pl.when(lead)
    def _():
        tell(barrier, x_dev)

    @pl.when(follow)
    def _():
        pl.semaphore_wait(barrier, 1)
        tell(hello, x_dev)

    @pl.when(lead)
    def _():
        pl.semaphore_wait(hello, 1)

    half_at = (pl.multiple_of((1 - y) * 2 * BLOCK, 2 * BLOCK), pl.multiple_of(y * 2 * BLOCK, 2 * BLOCK))

    def w_copy(which, own):
        ref = wts.at[which, my_z, pl.ds(half_at[own], 2 * BLOCK)]
        return remote(ref, ref, w_send, w_recv.at[which, own], x_dev)

    for which in (1, 0):
        loads[1 - which].wait()
        for own in range(2):
            w_copy(which, own).start()

    for rel in range(3):

        @pl.when(jnp.logical_and(lead, mates[rel] != 1))
        def _():
            tell(barrier, mate_dev(rel))

    @pl.when(plain)
    def _():
        pl.semaphore_wait(barrier, 3)
        tell(quad_ok, dev(i, z * 4 + 1))
        tell(hello, x_dev)

    @pl.when(herald)
    def _():
        pl.semaphore_wait(quad_ok, 3)
        tell(hello, x_dev)
        for q in range(1, nz):
            tell(barrier, z_dev(q))

    @pl.when(follow)
    def _():
        pl.semaphore_wait(hello, 1)

    others = [dev(i, lax.rem(j + k, n_dp)) for k in range(1, n_dp)]

    def hand_on(which, part_z, rel):
        at = pl.multiple_of(mates[rel] * BLOCK, BLOCK)
        send(wts.at[which, part_z, pl.ds(at, BLOCK)], wq.at[which, me, part_z], q_send, q_recv, mate_dev(rel))

    def keep_own(which, part_z):
        at = pl.multiple_of(me * BLOCK, BLOCK)
        wq[which, me, part_z] = wts[which, part_z, pl.ds(at, BLOCK)]

    for which in (1, 0):
        for rel in (1, 2, 0):
            hand_on(which, my_z, rel)

    keep = lax.broadcasted_iota(jnp.int32, (BLOCK, BLOCK), 1) <= lax.broadcasted_iota(
        jnp.int32, (BLOCK, BLOCK), 0
    )
    for load in loads[2:]:
        load.wait()
    spatial = jnp.where(keep, mix_ref[0].astype(f32), 0.0).astype(bf16)
    gain = gain_ref[...]
    bias = jnp.broadcast_to(bias_ref[...], (BLOCK, BLOCK)).T
    both = jnp.concatenate([wts[which, my_z].reshape(shard, BLOCK) for which in range(2)], axis=1)
    own = dot(hid[:, pl.ds(mine, shard)], both, 1, 0)
    pre_acc[0] = own[:, 0:BLOCK]
    pre_acc[1] = own[:, BLOCK:2 * BLOCK]
    for b in range(hid.shape[1] // BLOCK):
        hid_t[pl.ds(b * BLOCK, BLOCK), :] = hid[:, pl.ds(b * BLOCK, BLOCK)].T
    for which in range(2):
        keep_own(which, my_z)

    def finish(which, own):
        w_copy(which, own).wait_recv()
        part_sum = pre_acc[which]
        for zz in range(zs):
            at = pl.multiple_of(theirs + zz * 4 * BLOCK + half_at[own], 2 * BLOCK)
            part_sum = part_sum + dot(
                hid[:, pl.ds(at, 2 * BLOCK)],
                wts[which, zs * x_peer + zz, pl.ds(half_at[own], 2 * BLOCK)], 1, 0,
            )
        pre_acc[which] = part_sum

    def share(n, src, dst):
        for k, target in enumerate(others):
            send(src, dst.at[k], a_send.at[n], a_recv.at[n], target)

    def gather(n, src, dst):
        await_bytes(dst, a_recv.at[n])
        total = src[...]
        for k in range(len(others)):
            total = total + dst[k]
        return total * (1.0 / full_width)

    finish(1, 0)
    for rel in (1, 2):
        hand_on(1, their_z, rel)
    finish(1, 1)
    for k in range(chunks):
        rows = pl.ds(k * BLOCK, BLOCK)
        pre = pre_acc[1, rows, :].astype(bf16).astype(f32)
        cumulative, slope = phi_and_slope(pre)
        gating = pre * cumulative
        gat[rows, :] = gating
        slope_g[rows, :] = slope
        turned = gating.T
        gat_t[rows, :] = turned
        s1[k:k + 1, :] = jnp.sum(turned, axis=0, keepdims=True)
        s1[chunks + k:chunks + k + 1, :] = jnp.sum(turned * turned, axis=0, keepdims=True)

    @pl.when(herald)
    def _():
        pl.semaphore_wait(barrier, nz - 1)
        for rel in range(3):
            tell(all_ok, mate_dev(rel))
            tell(all_ok, dev(x_peer, z * 4 + mates[rel]))
        tell(all_ok, x_dev)

    @pl.when(jnp.logical_not(herald))
    def _():
        pl.semaphore_wait(all_ok, 1)

    share(0, s1, r1)
    hand_on(1, their_z, 0)
    keep_own(1, their_z)

    finish(0, 0)
    for rel in (1, 2):
        hand_on(0, their_z, rel)
    finish(0, 1)
    for k in range(chunks):
        rows = pl.ds(k * BLOCK, BLOCK)
        pre = pre_acc[0, rows, :].astype(bf16).astype(f32)
        wide = og[rows, :].astype(f32)
        cumulative, slope = phi_and_slope(pre)
        cs[rows, :] = wide * slope
        mixed_grad = (wide * (pre * cumulative)).astype(bf16)
        mg[rows, :] = mixed_grad
        centred_grad = dot(spatial, mixed_grad, 0, 0) * gain
        cg[rows, :] = centred_grad
        turned = centred_grad.T
        s2[k:k + 1, :] = jnp.sum(turned, axis=0, keepdims=True)
        s2[chunks + k:chunks + k + 1, :] = jnp.sum(turned * gat_t[rows, :], axis=0, keepdims=True)
    share(1, s2, r2)
    hand_on(0, their_z, 0)
    keep_own(0, their_z)

    def spread(row):
        return jnp.broadcast_to(row, (BLOCK, BLOCK)).T

    def exchange(which, k):
        ref = eq.at[which, me, pl.ds(k * BLOCK, BLOCK)]
        y_sem = yg_recv.at[k] if which else c_recv.at[0]
        s_sem = sg_recv.at[k] if which else c_recv.at[1]
        send(ref, ref, e_send, y_sem, mate_dev(1))
        send(ref, ref, e_send, s_sem, mate_dev(0))

    def all_terms(which, k):
        rows = pl.ds(k * BLOCK, BLOCK)
        grads = jnp.concatenate([eq[which, q, rows, :] for q in range(4)], axis=1)
        weights = jnp.concatenate([wq[which, q].reshape(nz * BLOCK, BLOCK) for q in range(4)], axis=1)
        return dot(grads, weights, 1, 1)

    t1 = gather(0, s1, r1)
    means, invs = [], []
    mixing = jnp.zeros((BLOCK, BLOCK), f32)
    for k in range(chunks):
        rows = pl.ds(k * BLOCK, BLOCK)
        mean = t1[k:k + 1]
        inv = lax.rsqrt(t1[chunks + k:chunks + k + 1] - mean * mean + norm_eps)
        means.append(mean)
        invs.append(inv)
        inv_w = spread(inv)
        centred = (gat[rows, :] - spread(mean)) * inv_w
        centred_ref[rows, :] = centred
        slope_g[rows, :] = slope_g[rows, :] * inv_w
        normed = (centred * gain).astype(bf16)
        mixed = dot(spatial, normed, 1, 0) + bias
        eq[0, me, rows, :] = (cs[rows, :] * mixed).astype(bf16)
        exchange(0, k)
        mixing = mixing + dot(mg[rows, :], normed, 1, 1)
    mixing = jnp.where(keep, mixing, 0.0)

    def weight_part(which, t):
        at = pl.multiple_of(theirs + t * tile, tile)
        rows = pl.ds(t * tile, tile)
        gs[which, rows, :] = dot(hid_t[pl.ds(at, tile), :], eq[which, me], 1, 0).astype(bf16)
        send(gs.at[which, rows], gr.at[which, rows], gx_send.at[which], gx_recv.at[which], x_dev)

    outs = (c_out, g_out)

    def weight_own(which, t):
        at = pl.multiple_of(mine + t * tile, tile)
        outs[which][pl.ds(t * tile, tile), :] = dot(hid_t[pl.ds(at, tile), :], eq[which, me], 1, 0)

    last = pl.ds(shard, BLOCK)
    gs[0, last, :] = mixing.astype(bf16)
    send(gs.at[0, last], gr.at[0, last], gx_send.at[0], gx_recv.at[0], x_dev)
    for t in range(chunks):
        weight_part(0, t)
    for t in range(chunks):
        weight_own(0, t)

    t2 = gather(1, s2, r2)
    for k in range(chunks):
        rows = pl.ds(k * BLOCK, BLOCK)
        first = t2[k:k + 1]
        second = invs[k] * (t2[chunks + k:chunks + k + 1] - means[k] * first)
        back = cg[rows, :] - spread(first) - centred_ref[rows, :] * spread(second)
        eq[1, me, rows, :] = (back * slope_g[rows, :]).astype(bf16)
        exchange(1, k)
    await_bytes(eq.at[0, 0], c_recv.at[0])
    handed = eq.at[0, y_mate]
    send(handed, handed, e_send, c_recv.at[1], mate_dev(0))
    await_bytes(wq.at[:, pl.ds(0, 3)], q_recv)
    await_bytes(eq.at[0, pl.ds(0, 2)], c_recv.at[1])
    for k in range(chunks):
        res = all_terms(0, k)
        for q in range(nz):
            part[k, q] = res[:, q * BLOCK:(q + 1) * BLOCK]

    def z_go(slot, k, rsem, land, q):
        send(z_send.at[slot, k], r_z.at[land, k], zz_send, rsem, z_dev(q))

    def pass_on(k):
        rows = pl.ds(k * BLOCK, BLOCK)
        await_bytes(eq.at[1, 0, rows], yg_recv.at[k])
        ref = eq.at[1, y_mate, rows]
        send(ref, ref, e_send, sg_recv.at[k], mate_dev(0))

    def spread_out(k):
        await_bytes(eq.at[1, pl.ds(0, 2), pl.ds(k * BLOCK, BLOCK)], sg_recv.at[k])
        res = all_terms(1, k)
        for q in range(nz):
            part[k, q] = part[k, q] + res[:, q * BLOCK:(q + 1) * BLOCK]
        z_send[0, k] = part[k, z_xor[3]].astype(bf16)

        @pl.when(mid == 0)
        def _():
            z_go(0, k, relay_recv.at[k], 3, 1)

        @pl.when(mid == 1)
        def _():
            z_go(0, k, zz_recv.at[0], 0, 3)
            z_send[2, k] = part[k, z_xor[1]].astype(bf16)
            z_go(2, k, zz_recv.at[1], 2, 1)

    def relay(k):
        @pl.when(mid == 1)
        def _():
            await_bytes(r_z.at[3, k], relay_recv.at[k])
            z_send[1, k] = (part[k, z_xor[2]] + r_z[3, k].astype(f32)).astype(bf16)
            z_go(1, k, zz_recv.at[1], 1, 2)

        @pl.when(mid == 0)
        def _():
            z_send[1, k] = part[k, z_xor[2]].astype(bf16)
            z_go(1, k, zz_recv.at[1], 1, 2)
            z_send[2, k] = part[k, z_xor[1]].astype(bf16)
            z_go(2, k, zz_recv.at[1], 2, 1)

    for step in range(chunks + 1):
        if step < chunks:
            pass_on(step)
        if step >= 1:
            spread_out(step - 1)
            weight_part(1, step - 1)
    for k in range(chunks):
        relay(k)
        weight_own(1, k)

    for which in range(2):
        rows = pl.ds(0, shard + (1 - which) * BLOCK)
        await_bytes(gr.at[which, rows], gx_recv.at[which])
        for t in range(chunks):
            rows = pl.ds(t * tile, tile)
            outs[which][rows, :] = (outs[which][rows, :] + gr[which, rows, :].astype(f32)) * grad_scale
        if which == 0:
            m_out[0] = (mixing + gr[0, last, :].astype(f32)) * grad_scale

    @pl.when(mid == 1)
    def _():
        await_bytes(r_z.at[0], zz_recv.at[0])
        for k in range(chunks):
            part[k, z] = part[k, z] + r_z[0, k].astype(f32)

    await_bytes(r_z.at[pl.ds(1, 2)], zz_recv.at[1])
    for k in range(chunks):
        x_out[pl.ds(k * BLOCK, BLOCK), :] = (
            part[k, z] + r_z[1, k].astype(f32) + r_z[2, k].astype(f32)
        ).astype(bf16)
    await_bytes(wts.at[:, my_z], w_send)
    await_bytes(wq.at[:, pl.ds(0, 3)], q_send)
    await_bytes(r1, a_send.at[0])
    await_bytes(r2, a_send.at[1])
    await_bytes(eq.at[:, pl.ds(0, 3)], e_send)
    await_bytes(gs.at[0], gx_send.at[0])
    await_bytes(gs.at[1, pl.ds(0, shard)], gx_send.at[1])
    await_bytes(z_send, zz_send)


def store_kernel(*refs):
    count = len(refs) // 2
    src, dst, sem = refs[:count], refs[count:2 * count], refs[-1]
    stores = [pltpu.make_async_copy(src[k], dst[k], sem.at[k]) for k in range(count)]
    for store in stores:
        store.start()
    for store in stores:
        store.wait()


def fused(n_dp, hidden_in, content_weight, gating_weight, norm_gain, mixing_weight, mixing_bias, out_grad):
    toks, depth = hidden_in.shape
    shard, width = content_weight.shape
    nz = n_dp // 4
    zs = nz // 2
    chunks = toks // BLOCK
    grad_scale = 1.0 / math.sqrt(2 * toks)
    bf16, f32 = jnp.bfloat16, jnp.float32
    in_hbm = pl.BlockSpec(memory_space=pltpu.HBM)
    dma = pltpu.SemaphoreType.DMA
    once = pltpu.SemaphoreType.REGULAR
    V = pltpu.VMEM
    wide = V((toks, width), f32)
    sums = V((2 * chunks, BLOCK), f32)
    sums_in = V((n_dp - 1, 2 * chunks, BLOCK), f32)
    scratch = [
        V((1, width), f32), V((1, BLOCK, BLOCK), bf16), V((1, BLOCK), f32),
        V((toks, depth), bf16), V((depth, toks), bf16), V((2, nz, 4 * BLOCK, width), bf16),
        V((2, 4, nz, BLOCK, width), bf16), V((toks, width), bf16), V((2, toks, width), f32),
        wide, wide, wide, wide, V((toks, width), bf16), wide, wide,
        V((2, 4, toks, width), bf16), V((chunks, nz, BLOCK, width), f32),
        sums, sums_in, sums, sums_in,
        V((nz - 1, chunks, BLOCK, width), bf16), V((nz, chunks, BLOCK, width), bf16),
        V((2, shard + BLOCK, width), bf16), V((2, shard + BLOCK, width), bf16),
        dma((7,)), once, once, once, dma, dma((2, 2)), dma, dma, dma((2,)), dma((2,)),
        dma, dma((2,)), dma((chunks,)), dma((chunks,)), dma((2,)), dma((2,)), dma, dma((2,)), dma((chunks,)),
    ]
    in_vmem = pl.BlockSpec(memory_space=V)
    results = pl.pallas_call(
        functools.partial(fused_kernel, n_dp, width * n_dp, grad_scale),
        out_shape=(
            V((toks, width), bf16),
            V((shard, width), f32),
            V((shard, width), f32),
            V(mixing_weight.shape, f32),
        ),
        in_specs=[in_hbm] * 7,
        out_specs=(in_vmem,) * 4,
        scratch_shapes=scratch,
        compiler_params=pltpu.CompilerParams(
            collective_id=0, has_side_effects=True, vmem_limit_bytes=60 * 1024 * 1024
        ),
    )(
        hidden_in, content_weight.reshape(zs, 4 * BLOCK, width), gating_weight.reshape(zs, 4 * BLOCK, width),
        norm_gain[None, :], mixing_weight, mixing_bias, out_grad,
    )
    return pl.pallas_call(
        store_kernel,
        out_shape=tuple(jax.ShapeDtypeStruct(r.shape, r.dtype) for r in results),
        in_specs=[in_vmem] * 4,
        out_specs=(in_hbm,) * 4,
        scratch_shapes=[dma((4,))],
        compiler_params=pltpu.CompilerParams(vmem_limit_bytes=60 * 1024 * 1024),
    )(*[pltpu.with_memory_space_constraint(r, V) for r in results])


def fits(n_sp, n_dp, toks, shard, width):
    paired = n_sp == 2 and n_dp == 16
    return paired and width == GROUP_DIM and shard == 2 * 4 * BLOCK and toks == 4 * BLOCK


def solve(*args):
    n_sp, n_dp = lax.axis_size("sp"), lax.axis_size("dp")
    shard, width = args[1].shape
    if fits(n_sp, n_dp, args[0].shape[0], shard, width) and args[0].shape[1] == n_dp * width:
        return fused(n_dp, *args)
    return local(*args)


def solution(mesh):
    in_specs = (
        P("sp", None),
        P("sp", "dp"),
        P("sp", "dp"),
        P("dp"),
        P("dp", None, None),
        P("dp", None),
        P("sp", "dp"),
    )
    out_specs = (P("sp", "dp"), P("sp", "dp"), P("sp", "dp"), P("dp", None, None))
    return jax.shard_map(solve, mesh=mesh, in_specs=in_specs, out_specs=out_specs, check_vma=False)
```

time: 43.1 us -> 39.4 us (0.914)
  Pallas kernels: 42.3 us -> 38.7 us
    pallas_call x1, Pallas kernels: 41.2 us -> 37.6 us  [fused(): pl.pallas_call(functools.partial(fused_kernel, n_dp, width * n_dp, grad_s...]
where the time goes in v3:
time: 39.4 us; the launch traced here: 39.3 us
  Pallas kernels  38.7 us (98%)
  between operations  0.64 us (2%)
    pallas_call x1, Pallas kernels, fused(): pl.pallas_call(functools.partial(fused_kernel, n_dp, width * n_dp, grad_s...  37.6 us
    pallas_call x1, Pallas kernels, fused(): pl.pallas_call(store_kernel, out_shape=tuple((jax.ShapeDtypeStruct(r.shap...  1.06 us

profile of v3, /device:TPU:0, one launch (start us, length us, event | category | flops | bytes accessed | tf_op | source)
XLA Modules:
  0.0 39.3 jit_solution(4830440854666046771)
XLA Ops:
  0.6 37.6 %shard_map.102 = (bf16[512,128]{1,0:T(8,128)(2,1)S(1)}, f32[1024,128]{1,0:T(8,128)S(1)}, f32[1024,128]{1,0:T(8,128)S(1)}, f32[1,128,128]{2,1,0:T(8,128)S(1)}) custom-call(bf16[512,2048]{1,0:T(8,128)(2,1)} %h_in.1, bf16[2,512,128]{2,1,0:T(8,128)(2,1)} %bitcast.3, bf16[2,512,128]{2,1,0:T(8,128)(2,1)} %bitcast.4, f32[1,128]{1,0:T(1,128)} %bitcast.5, ...), custom_call_target="tpu_custom_call" | custom-call | tf_op jit(solution)/shard_map/pallas_call | solution.py:550
  38.2 1.1 %shard_map.103 = (bf16[512,128]{1,0:T(8,128)(2,1)}, f32[1024,128]{1,0:T(8,128)}, f32[1024,128]{1,0:T(8,128)}, f32[1,128,128]{2,1,0:T(8,128)}) custom-call(bf16[512,128]{1,0:T(8,128)(2,1)S(1)} %get-tuple-element.8.refs_0_, f32[1024,128]{1,0:T(8,128)S(1)} %get-tuple-element.9.refs_1_, f32[1024,128]{1,0:T(8,128)S(1)} %get-tuple-element.10.refs_2_, ...), custom_call_target="tpu_custom_call" | custom-call | tf_op jit(solution)/shard_map/pallas_call | solution.py:568

commit v4 on v3

--- a/solution.py
+++ b/solution.py
@@ -223,8 +223,13 @@
 
     for which in (1, 0):
         loads[1 - which].wait()
-        for own in range(2):
-            w_copy(which, own).start()
+        w_copy(which, 0).start()
+        if which == 1:
+            w_copy(1, 1).start()
+
+    @pl.when(c == 0)
+    def _():
+        w_copy(0, 1).start()
 
     for rel in range(3):
 
@@ -306,6 +311,11 @@
     for rel in (1, 2):
         hand_on(1, their_z, rel)
     finish(1, 1)
+
+    @pl.when(c == 1)
+    def _():
+        w_copy(0, 1).start()
+
     for k in range(chunks):
         rows = pl.ds(k * BLOCK, BLOCK)
         pre = pre_acc[1, rows, :].astype(bf16).astype(f32)
@@ -419,9 +429,53 @@
         back = cg[rows, :] - spread(first) - centred_ref[rows, :] * spread(second)
         eq[1, me, rows, :] = (back * slope_g[rows, :]).astype(bf16)
         exchange(1, k)
+    for t in range(chunks):
+        weight_part(1, t)
     await_bytes(eq.at[0, 0], c_recv.at[0])
     handed = eq.at[0, y_mate]
     send(handed, handed, e_send, c_recv.at[1], mate_dev(0))
+    for t in range(chunks):
+        weight_own(1, t)
+
+    def z_go(slot, k, land, rsem, q):
+        send(z_send.at[slot, k], r_z.at[land, k], zz_send, rsem, z_dev(q))
+
+    def pass_on(k):
+        rows = pl.ds(k * BLOCK, BLOCK)
+        await_bytes(eq.at[1, 0, rows], yg_recv.at[k])
+        ref = eq.at[1, y_mate, rows]
+        send(ref, ref, e_send, sg_recv.at[k], mate_dev(0))
+
+    def spread_out(k):
+        await_bytes(eq.at[1, pl.ds(0, 2), pl.ds(k * BLOCK, BLOCK)], sg_recv.at[k])
+        res = all_terms(1, k)
+        for q in range(nz):
+            part[k, q] = part[k, q] + res[:, q * BLOCK:(q + 1) * BLOCK]
+
+        @pl.when(mid == 0)
+        def _():
+            for slot in range(2):
+                z_send[slot, k] = part[k, z_xor[3 - slot]].astype(bf16)
+                z_go(slot, k, 2 + slot, relay_recv.at[slot, k], 1)
+
+        @pl.when(mid == 1)
+        def _():
+            near_end(k)
+
+    def near_end(k):
+        z_send[2, k] = part[k, z_xor[1]].astype(bf16)
+        z_go(2, k, 1, zz_recv, 1)
+
+    def relay(k):
+        for slot in range(2):
+            await_bytes(r_z.at[2 + slot, k], relay_recv.at[slot, k])
+            z_send[1 - slot, k] = (part[k, z_xor[2 + slot]] + r_z[2 + slot, k].astype(f32)).astype(bf16)
+            z_go(1 - slot, k, 0, zz_recv, 2 + slot)
+
+    @pl.when(c == 1)
+    def _():
+        pass_on(0)
+
     await_bytes(wq.at[:, pl.ds(0, 3)], q_recv)
     await_bytes(eq.at[0, pl.ds(0, 2)], c_recv.at[1])
     for k in range(chunks):
@@ -429,55 +483,27 @@
         for q in range(nz):
             part[k, q] = res[:, q * BLOCK:(q + 1) * BLOCK]
 
-    def z_go(slot, k, rsem, land, q):
-        send(z_send.at[slot, k], r_z.at[land, k], zz_send, rsem, z_dev(q))
-
-    def pass_on(k):
-        rows = pl.ds(k * BLOCK, BLOCK)
-        await_bytes(eq.at[1, 0, rows], yg_recv.at[k])
-        ref = eq.at[1, y_mate, rows]
-        send(ref, ref, e_send, sg_recv.at[k], mate_dev(0))
-
-    def spread_out(k):
-        await_bytes(eq.at[1, pl.ds(0, 2), pl.ds(k * BLOCK, BLOCK)], sg_recv.at[k])
-        res = all_terms(1, k)
-        for q in range(nz):
-            part[k, q] = part[k, q] + res[:, q * BLOCK:(q + 1) * BLOCK]
-        z_send[0, k] = part[k, z_xor[3]].astype(bf16)
-
-        @pl.when(mid == 0)
+    @pl.when(c == 1)
+    def _():
+        for k in range(1, chunks):
+            pass_on(k)
+
+    for k in range(chunks):
+
+        @pl.when(c == 0)
         def _():
-            z_go(0, k, relay_recv.at[k], 3, 1)
-
-        @pl.when(mid == 1)
-        def _():
-            z_go(0, k, zz_recv.at[0], 0, 3)
-            z_send[2, k] = part[k, z_xor[1]].astype(bf16)
-            z_go(2, k, zz_recv.at[1], 2, 1)
-
-    def relay(k):
-        @pl.when(mid == 1)
-        def _():
-            await_bytes(r_z.at[3, k], relay_recv.at[k])
-            z_send[1, k] = (part[k, z_xor[2]] + r_z[3, k].astype(f32)).astype(bf16)
-            z_go(1, k, zz_recv.at[1], 1, 2)
-
-        @pl.when(mid == 0)
-        def _():
-            z_send[1, k] = part[k, z_xor[2]].astype(bf16)
-            z_go(1, k, zz_recv.at[1], 1, 2)
-            z_send[2, k] = part[k, z_xor[1]].astype(bf16)
-            z_go(2, k, zz_recv.at[1], 2, 1)
-
-    for step in range(chunks + 1):
-        if step < chunks:
-            pass_on(step)
-        if step >= 1:
-            spread_out(step - 1)
-            weight_part(1, step - 1)
-    for k in range(chunks):
-        relay(k)
-        weight_own(1, k)
+            pass_on(k)
+
+        spread_out(k)
+    @pl.when(mid == 1)
+    def _():
+        for k in range(chunks):
+            relay(k)
+
+    @pl.when(mid == 0)
+    def _():
+        for k in range(chunks):
+            near_end(k)
 
     for which in range(2):
         rows = pl.ds(0, shard + (1 - which) * BLOCK)
@@ -488,16 +514,10 @@
         if which == 0:
             m_out[0] = (mixing + gr[0, last, :].astype(f32)) * grad_scale
 
-    @pl.when(mid == 1)
-    def _():
-        await_bytes(r_z.at[0], zz_recv.at[0])
-        for k in range(chunks):
-            part[k, z] = part[k, z] + r_z[0, k].astype(f32)
-
-    await_bytes(r_z.at[pl.ds(1, 2)], zz_recv.at[1])
+    await_bytes(r_z.at[pl.ds(0, 2)], zz_recv)
     for k in range(chunks):
         x_out[pl.ds(k * BLOCK, BLOCK), :] = (
-            part[k, z] + r_z[1, k].astype(f32) + r_z[2, k].astype(f32)
+            part[k, z] + r_z[0, k].astype(f32) + r_z[1, k].astype(f32)
         ).astype(bf16)
     await_bytes(wts.at[:, my_z], w_send)
     await_bytes(wq.at[:, pl.ds(0, 3)], q_send)
@@ -544,7 +564,7 @@
         V((nz - 1, chunks, BLOCK, width), bf16), V((nz, chunks, BLOCK, width), bf16),
         V((2, shard + BLOCK, width), bf16), V((2, shard + BLOCK, width), bf16),
         dma((7,)), once, once, once, dma, dma((2, 2)), dma, dma, dma((2,)), dma((2,)),
-        dma, dma((2,)), dma((chunks,)), dma((chunks,)), dma((2,)), dma((2,)), dma, dma((2,)), dma((chunks,)),
+        dma, dma((2,)), dma((chunks,)), dma((chunks,)), dma((2,)), dma((2,)), dma, dma, dma((2, chunks)),
     ]
     in_vmem = pl.BlockSpec(memory_space=V)
     results = pl.pallas_call(

time: 39.4 us -> 39.1 us (level)
  Pallas kernels: 38.7 us -> 38.3 us
where the time goes in v4:
time: 39.1 us; the launch traced here: 38.9 us
  Pallas kernels  38.3 us (98%)
  between operations  0.64 us (2%)
    pallas_call x1, Pallas kernels, fused(): pl.pallas_call(functools.partial(fused_kernel, n_dp, width * n_dp, grad_s...  37.2 us
    pallas_call x1, Pallas kernels, fused(): pl.pallas_call(store_kernel, out_shape=tuple((jax.ShapeDtypeStruct(r.shap...  1.06 us

profile of v4, /device:TPU:0, one launch (start us, length us, event | category | flops | bytes accessed | tf_op | source)
XLA Modules:
  0.0 38.9 jit_solution(8389840006947353056)
XLA Ops:
  0.6 37.2 %shard_map.102 = (bf16[512,128]{1,0:T(8,128)(2,1)S(1)}, f32[1024,128]{1,0:T(8,128)S(1)}, f32[1024,128]{1,0:T(8,128)S(1)}, f32[1,128,128]{2,1,0:T(8,128)S(1)}) custom-call(bf16[512,2048]{1,0:T(8,128)(2,1)} %h_in.1, bf16[2,512,128]{2,1,0:T(8,128)(2,1)} %bitcast.3, bf16[2,512,128]{2,1,0:T(8,128)(2,1)} %bitcast.4, f32[1,128]{1,0:T(1,128)} %bitcast.5, ...), custom_call_target="tpu_custom_call" | custom-call | tf_op jit(solution)/shard_map/pallas_call | solution.py:570
  37.9 1.1 %shard_map.103 = (bf16[512,128]{1,0:T(8,128)(2,1)}, f32[1024,128]{1,0:T(8,128)}, f32[1024,128]{1,0:T(8,128)}, f32[1,128,128]{2,1,0:T(8,128)}) custom-call(bf16[512,128]{1,0:T(8,128)(2,1)S(1)} %get-tuple-element.8.refs_0_, f32[1024,128]{1,0:T(8,128)S(1)} %get-tuple-element.9.refs_1_, f32[1024,128]{1,0:T(8,128)S(1)} %get-tuple-element.10.refs_2_, ...), custom_call_target="tpu_custom_call" | custom-call | tf_op jit(solution)/shard_map/pallas_call | solution.py:588

commit v5 on v4

--- a/solution.py
+++ b/solution.py
@@ -418,9 +418,6 @@
     send(gs.at[0, last], gr.at[0, last], gx_send.at[0], gx_recv.at[0], x_dev)
     for t in range(chunks):
         weight_part(0, t)
-    for t in range(chunks):
-        weight_own(0, t)
-
     t2 = gather(1, s2, r2)
     for k in range(chunks):
         rows = pl.ds(k * BLOCK, BLOCK)
@@ -436,6 +433,7 @@
     send(handed, handed, e_send, c_recv.at[1], mate_dev(0))
     for t in range(chunks):
         weight_own(1, t)
+        weight_own(0, t)
 
     def z_go(slot, k, land, rsem, q):
         send(z_send.at[slot, k], r_z.at[land, k], zz_send, rsem, z_dev(q))

time: 39.1 us -> 39 us (level)
  no operation moved by 1% of the time
where the time goes in v5:
time: 39 us; the launch traced here: 38.8 us
  Pallas kernels  38.2 us (98%)
  between operations  0.64 us (2%)
    pallas_call x1, Pallas kernels, fused(): pl.pallas_call(functools.partial(fused_kernel, n_dp, width * n_dp, grad_s...  37.1 us
    pallas_call x1, Pallas kernels, fused(): pl.pallas_call(store_kernel, out_shape=tuple((jax.ShapeDtypeStruct(r.shap...  1.06 us

profile of v5, /device:TPU:0, one launch (start us, length us, event | category | flops | bytes accessed | tf_op | source)
XLA Modules:
  0.0 38.8 jit_solution(2772664845646306284)
XLA Ops:
  0.6 37.1 %shard_map.102 = (bf16[512,128]{1,0:T(8,128)(2,1)S(1)}, f32[1024,128]{1,0:T(8,128)S(1)}, f32[1024,128]{1,0:T(8,128)S(1)}, f32[1,128,128]{2,1,0:T(8,128)S(1)}) custom-call(bf16[512,2048]{1,0:T(8,128)(2,1)} %h_in.1, bf16[2,512,128]{2,1,0:T(8,128)(2,1)} %bitcast.3, bf16[2,512,128]{2,1,0:T(8,128)(2,1)} %bitcast.4, f32[1,128]{1,0:T(1,128)} %bitcast.5, ...), custom_call_target="tpu_custom_call" | custom-call | tf_op jit(solution)/shard_map/pallas_call | solution.py:568
  37.8 1.1 %shard_map.103 = (bf16[512,128]{1,0:T(8,128)(2,1)}, f32[1024,128]{1,0:T(8,128)}, f32[1024,128]{1,0:T(8,128)}, f32[1,128,128]{2,1,0:T(8,128)}) custom-call(bf16[512,128]{1,0:T(8,128)(2,1)S(1)} %get-tuple-element.8.refs_0_, f32[1024,128]{1,0:T(8,128)S(1)} %get-tuple-element.9.refs_1_, f32[1024,128]{1,0:T(8,128)S(1)} %get-tuple-element.10.refs_2_, ...), custom_call_target="tpu_custom_call" | custom-call | tf_op jit(solution)/shard_map/pallas_call | solution.py:586

commit v6 on v5

--- a/solution.py
+++ b/solution.py
@@ -455,6 +455,8 @@
             for slot in range(2):
                 z_send[slot, k] = part[k, z_xor[3 - slot]].astype(bf16)
                 z_go(slot, k, 2 + slot, relay_recv.at[slot, k], 1)
+            if k == 0:
+                near_end(k)
 
         @pl.when(mid == 1)
         def _():
@@ -500,7 +502,7 @@
 
     @pl.when(mid == 0)
     def _():
-        for k in range(chunks):
+        for k in range(1, chunks):
             near_end(k)
 
     for which in range(2):

time: 39 us -> 39.1 us (level)
  no operation moved by 1% of the time
where the time goes in v6:
time: 39.1 us; the launch traced here: 39 us
  Pallas kernels  38.4 us (98%)
  between operations  0.64 us (2%)
    pallas_call x1, Pallas kernels, fused(): pl.pallas_call(functools.partial(fused_kernel, n_dp, width * n_dp, grad_s...  37.3 us
    pallas_call x1, Pallas kernels, fused(): pl.pallas_call(store_kernel, out_shape=tuple((jax.ShapeDtypeStruct(r.shap...  1.06 us

profile of v6, /device:TPU:0, one launch (start us, length us, event | category | flops | bytes accessed | tf_op | source)
XLA Modules:
  0.0 39.0 jit_solution(18425255284174342856)
XLA Ops:
  0.6 37.3 %shard_map.102 = (bf16[512,128]{1,0:T(8,128)(2,1)S(1)}, f32[1024,128]{1,0:T(8,128)S(1)}, f32[1024,128]{1,0:T(8,128)S(1)}, f32[1,128,128]{2,1,0:T(8,128)S(1)}) custom-call(bf16[512,2048]{1,0:T(8,128)(2,1)} %h_in.1, bf16[2,512,128]{2,1,0:T(8,128)(2,1)} %bitcast.3, bf16[2,512,128]{2,1,0:T(8,128)(2,1)} %bitcast.4, f32[1,128]{1,0:T(1,128)} %bitcast.5, ...), custom_call_target="tpu_custom_call" | custom-call | tf_op jit(solution)/shard_map/pallas_call | solution.py:570
  37.9 1.1 %shard_map.103 = (bf16[512,128]{1,0:T(8,128)(2,1)}, f32[1024,128]{1,0:T(8,128)}, f32[1024,128]{1,0:T(8,128)}, f32[1,128,128]{2,1,0:T(8,128)}) custom-call(bf16[512,128]{1,0:T(8,128)(2,1)S(1)} %get-tuple-element.8.refs_0_, f32[1024,128]{1,0:T(8,128)S(1)} %get-tuple-element.9.refs_1_, f32[1024,128]{1,0:T(8,128)S(1)} %get-tuple-element.10.refs_2_, ...), custom_call_target="tpu_custom_call" | custom-call | tf_op jit(solution)/shard_map/pallas_call | solution.py:588
